TPU v7x, 32 devices: a whole 2x2x4 slice. The times are simulated.
32 devices in a mesh: grp: 2 (over y), sp: 4 (over z), tp: 4 (over x, core).
Axes of the slice: x: 2, y: 2, z: 4, core: 2. Of those that a mesh axis runs over, the one named last changes fastest.
Arguments:
- tokens: bfloat16 [3072, 2048], P(('grp', 'sp')), parts along dimension 0, may hold values from -6 to 6
- norm_gain: float32 [2048], replicated, may hold values from 0.1 to 1.9
- w_query: bfloat16 [2048, 1024], P(None, 'tp'), may hold values from -0.088388348 to 0.088388348
- w_key: bfloat16 [2048, 1024], P(None, 'tp'), may hold values from -1.5467961 to 1.5467961
- w_value: bfloat16 [2048, 1024], P(None, 'tp'), may hold values from -0.30935922 to 0.30935922
- out_gain: float32 [1024], P('tp'), may hold values from 0.1 to 1.9
- w_out: bfloat16 [1024, 2048], P('tp'), may hold values from -0.1875 to 0.1875
Outputs:
- mixed: bfloat16 [3072, 2048], P(('grp', 'sp', 'tp')), parts along dimension 0
There are 2 independent parts, one for each index of `grp`. A program takes and returns all parts, laid end to end along the dimension named above; an argument that names none is the same for every part. Nothing has to cross between parts.
All inputs are finite; a program needn't handle non-finite values.
Results may differ from a plain program's by a relative error of at most 0.015.
Values may be sent and summed in bfloat16 or wider, within the bound.
A program may use at most 64 MiB of HBM per device.

v0:
```python
from functools import reduce

import jax
import jax.numpy as jnp
from jax import lax
from jax.sharding import PartitionSpec as P

HEAD_DIM = 64
WINDOW_FIRST = 128
WINDOW_SECOND = 512
DILATION_SECOND = 4
WINDOW_THIRD = 2048
DILATION_THIRD = 16


EPS = 1e-06
NEG = -1e30


def from_behind(value, axis, steps):
    count = lax.axis_size(axis)
    initial, last = (max(0, -steps), min(count, count - steps))
    return lax.ppermute(value, axis, [(source, source + steps) for source in range(initial, last)])


def band_part(queries, key_rows, value_rows, span_len, dilation_step, first_key):
    query_len, head_count, head_width = queries.shape
    class_len = query_len // dilation_step
    block_len = class_len if class_len <= 128 else 128
    blocks = class_len // block_len
    window_len = block_len + span_len
    query_blk = queries.reshape(blocks, block_len, dilation_step, head_count, head_width)
    key_cls = key_rows.reshape(class_len + span_len, dilation_step, head_count, head_width)
    value_cls = value_rows.reshape(class_len + span_len, dilation_step, head_count, head_width)
    key_blk = jnp.stack(
        [
            key_cls[block_idx * block_len : block_idx * block_len + window_len]
            for block_idx in range(blocks)
        ]
    )
    value_blk = jnp.stack(
        [
            value_cls[block_idx * block_len : block_idx * block_len + window_len]
            for block_idx in range(blocks)
        ]
    )
    scores = jnp.einsum(
        "jqchx,jkchx->jchqk", query_blk, key_blk, preferred_element_type=jnp.float32
    ) * HEAD_DIM ** (-0.5)
    lag_steps = (
        span_len
        + jnp.arange(block_len, dtype=jnp.int32)[:, None]
        - jnp.arange(window_len, dtype=jnp.int32)[None, :]
    )
    inside = (lag_steps >= 0) & (lag_steps <= span_len)
    key_pos = (
        first_key
        + (
            jnp.arange(blocks, dtype=jnp.int32)[:, None, None] * block_len
            + jnp.arange(window_len, dtype=jnp.int32)[None, None, :]
        )
        * dilation_step
        + jnp.arange(dilation_step, dtype=jnp.int32)[None, :, None]
    )
    usable = inside[None, None, None] & (key_pos >= 0)[:, :, None, None, :]
    scores = jnp.where(usable, scores, NEG)
    row_max = jnp.max(scores, axis=-1)
    weights = jnp.exp(scores - row_max[..., None])
    row_sum = jnp.sum(weights, axis=-1)
    weighted = jnp.einsum(
        "jchqk,jkchx->jqchx",
        weights.astype(jnp.bfloat16),
        value_blk,
        preferred_element_type=jnp.float32,
    )
    weighted = weighted.reshape(query_len, head_count, head_width)
    row_max = jnp.transpose(row_max, (0, 3, 1, 2)).reshape(query_len, head_count)
    row_sum = jnp.transpose(row_sum, (0, 3, 1, 2)).reshape(query_len, head_count)
    return (weighted, row_max, row_sum)


def mixture(pattern_out):
    peak_max = reduce(jnp.maximum, [result[1] for result in pattern_out])
    numerator = reduce(
        lambda left, right: left + right,
        [jnp.exp(result[1] - peak_max)[..., None] * result[0] for result in pattern_out],
    )
    denominator = reduce(
        lambda left, right: left + right,
        [jnp.exp(result[1] - peak_max) * result[2] for result in pattern_out],
    )
    return numerator / denominator[..., None]


def on_device(tokens, norm_gain, w_query, w_key, w_value, out_gain, w_out):
    tok_rows = tokens.shape[0]
    inverse = lax.rsqrt(jnp.mean(jnp.square(tokens.astype(jnp.float32)), axis=-1) + EPS)
    scaled = (tokens * norm_gain).astype(jnp.bfloat16)

    def project(weight):
        return (
            jnp.dot(scaled, weight, preferred_element_type=jnp.float32) * inverse[:, None]
        ).astype(jnp.bfloat16)

    queries = project(w_query)
    key_rows = project(w_key)
    value_rows = project(w_value)
    channels = w_query.shape[1]
    head_count = channels // HEAD_DIM
    offset = lax.axis_index("sp") * tok_rows
    reach_devs = min(-(-WINDOW_THIRD // tok_rows), lax.axis_size("sp") - 1)
    key_value = (key_rows, value_rows)
    older_keys = []
    older_values = []
    current = key_value
    for distance in range(reach_devs):
        current = from_behind((current[0], current[1]), "sp", 1)
        older_keys.insert(0, current[0])
        older_values.insert(0, current[1])
    excess = reach_devs * tok_rows - WINDOW_THIRD
    if excess >= 0:
        far_keys = jnp.concatenate(older_keys, axis=0)[excess:]
        far_values = jnp.concatenate(older_values, axis=0)[excess:]
    else:
        padding = jnp.zeros((-excess, channels), jnp.bfloat16)
        far_keys = jnp.concatenate([padding] + older_keys, axis=0)
        far_values = jnp.concatenate([padding] + older_values, axis=0)
    query_heads = queries.reshape(tok_rows, head_count, HEAD_DIM)
    pattern_out = []
    for window_span, dilation_step in (
        (WINDOW_FIRST, 1),
        (WINDOW_SECOND, DILATION_SECOND),
        (WINDOW_THIRD, DILATION_THIRD),
    ):
        keys_ext = jnp.concatenate(
            [far_keys[WINDOW_THIRD - window_span :], key_rows], axis=0
        ).reshape(window_span + tok_rows, head_count, HEAD_DIM)
        values_ext = jnp.concatenate(
            [far_values[WINDOW_THIRD - window_span :], value_rows], axis=0
        ).reshape(window_span + tok_rows, head_count, HEAD_DIM)
        pattern_out.append(
            band_part(
                query_heads,
                keys_ext,
                values_ext,
                window_span // dilation_step,
                dilation_step,
                offset - window_span,
            )
        )
    attended = mixture(pattern_out).reshape(tok_rows, channels)
    squares = lax.psum(jnp.sum(attended * attended, axis=-1), "tp")
    out_scale = lax.rsqrt(squares / (channels * lax.axis_size("tp")) + EPS)
    gated = (attended * out_gain).astype(jnp.bfloat16)
    share_rows = tok_rows // lax.axis_size("tp")
    summed = lax.psum_scatter(
        jnp.dot(gated, w_out, preferred_element_type=jnp.float32).astype(jnp.bfloat16),
        "tp",
        scatter_dimension=0,
        tiled=True,
    ).astype(jnp.float32)
    own_scale = lax.dynamic_slice_in_dim(
        out_scale, lax.axis_index("tp") * share_rows, share_rows, 0
    )
    return (summed * own_scale[:, None]).astype(jnp.bfloat16)


def solution(mesh):
    in_specs = (
        P(("grp", "sp"), None),
        P(),
        P(None, "tp"),
        P(None, "tp"),
        P(None, "tp"),
        P("tp"),
        P("tp", None),
    )
    out_specs = P(("grp", "sp", "tp"), None)
    return jax.shard_map(
        on_device, mesh=mesh, in_specs=in_specs, out_specs=out_specs, check_vma=False
    )
```

profile of v0, /device:TPU:9, one launch (start us, length us, event | category | flops | bytes accessed | tf_op | source)
XLA Modules:
  0.0 134.2 jit_solution(11729658480590497459)
XLA Ops:
  6.5 1.9 %fusion.1 = f32[384]{0:T(512)S(1)} fusion(bf16[384,2048]{1,0:T(8,128)(2,1)} %param.7), kind=kLoop, calls=%fused_computation.3 | loop fusion | flops 2358912 | bytes 1574400 | tf_op jit(solution)/shard_map/reduce_sum | solution.py:97
  8.5 1.9 %fusion.26 = bf16[384,256]{1,0:T(8,128)(2,1)S(1)} fusion(bf16[2048,256]{1,0:T(8,128)(2,1)} %param.11, bf16[384,2048]{1,0:T(8,128)(2,1)S(1)} %copy-done.3, f32[2048]{0:T(1024)} %param.8, f32[384]{0:T(512)S(1)} %add_rsqrt_fusion.1), kind=kOutput, calls=%fused_computation.29 | convolution fusion | flops 405209088 | bytes 2827776 | tf_op jit(solution)/shard_map/dot_general | solution.py:102
  10.4 3.3 %collective-permute-start.3 = (bf16[384,256]{1,0:T(8,128)(2,1)S(1)}, bf16[384,256]{1,0:T(8,128)(2,1)S(1)}, u32[]{:S(2)}, u32[]{:S(2)}) collective-permute-start(bf16[384,256]{1,0:T(8,128)(2,1)S(1)} %fusion.26), channel_id=1, source_target_pairs={{0,4},{4,8},{8,12},{1,5},{5,9},{9,13},{2,6},{6,10},{10,14},{3,7},{... | collective-permute-start | bytes 589832 | tf_op jit(solution)/shard_map/ppermute | solution.py:23
  14.4 3.2 %collective-permute-start = (bf16[384,256]{1,0:T(8,128)(2,1)S(1)}, bf16[384,256]{1,0:T(8,128)(2,1)}, u32[]{:S(2)}, u32[]{:S(2)}) collective-permute-start(bf16[384,256]{1,0:T(8,128)(2,1)S(1)} %fusion.23), channel_id=1, source_target_pairs={{0,4},{4,8},{8,12},{1,5},{5,9},{9,13},{2,6},{6,10},{10,14},{3,7},{... | collective-permute-start | bytes 589832 | tf_op jit(solution)/shard_map/ppermute | solution.py:23
  18.2 1.0 reshape.480
  19.2 1.0 reshape.477
  20.2 1.0 reshape.500
  21.2 0.8 broadcast_dynamic-update-slice_fusion.1
  22.0 0.8 broadcast_dynamic-update-slice_fusion
  23.2 0.7 broadcast_and_fusion.2
  23.9 0.7 broadcast_and_fusion.1
  24.6 0.7 broadcast_and_fusion
  25.3 0.8 slice.52
  26.1 0.8 copy.99
  26.9 0.8 copy.101
  27.7 0.8 copy.100
  28.4 1.9 %collective-permute-start.1 = (bf16[384,256]{1,0:T(8,128)(2,1)}, bf16[384,256]{1,0:T(8,128)(2,1)S(1)}, u32[]{:S(2)}, u32[]{:S(2)}) collective-permute-start(bf16[384,256]{1,0:T(8,128)(2,1)} %collective-permute-done), channel_id=1, source_target_pairs={{0,4},{4,8},{8,12},{1,5},{5,9},{9,13},{2,6},{6,10},{10,14},{3,7},{... | collective-permute-start | bytes 589832 | tf_op jit(solution)/shard_map/ppermute | solution.py:23
  30.3 1.6 %fusion.78 = (f32[3,4,128]{2,1,0:T(4,128)S(1)}, f32[3,4,128,256]{3,2,1,0:T(8,128)S(1)}) fusion(bf16[1,256,1,4,64]{1,4,3,0,2:T(8,128)(2,1)} %bitcast.191, bf16[1,256,1,4,64]{1,4,3,0,2:T(8,128)(2,1)} %bitcast.192, bf16[1,256,1,4,64]{1,4,3,0,2:T(8,128)(2,1)} %bitcast.190, bf16[3,128,4,64]{3,2,1,0:T(4,128)(2,1)} %reshape.500, ...), kind=kOutput, calls=%fused_computation.124 | convolution fusion | flops 51902976 | bytes 2267136 | tf_op jit(solution)/shard_map/jqchx,jkchx->jchqk/dot_general | solution.py:47
  32.0 0.8 pad_maximum_fusion.2
  32.8 1.7 %copy.113 = bf16[256,256]{0,1:T(8,128)(2,1)} copy(bf16[256,256]{1,0:T(8,128)(2,1)} %get-tuple-element.13) | data formatting | bytes 262144 | tf_op jit(solution)/shard_map/slice | solution.py:43
  34.5 1.7 %copy.115 = bf16[256,256]{0,1:T(8,128)(2,1)} copy(bf16[256,256]{1,0:T(8,128)(2,1)} %get-tuple-element.14) | data formatting | bytes 262144 | tf_op jit(solution)/shard_map/slice | solution.py:43
  36.2 0.8 copy.114
  36.9 1.9 %collective-permute-start.4 = (bf16[384,256]{1,0:T(8,128)(2,1)S(1)}, bf16[384,256]{1,0:T(8,128)(2,1)}, u32[]{:S(2)}, u32[]{:S(2)}) collective-permute-start(bf16[384,256]{1,0:T(8,128)(2,1)S(1)} %collective-permute-done.3), channel_id=1, source_target_pairs={{0,4},{4,8},{8,12},{1,5},{5,9},{9,13},{2,6},{6,10},{10,14},{3,7},{... | collective-permute-start | bytes 589832 | tf_op jit(solution)/shard_map/ppermute | solution.py:23
  38.8 1.1 fusion.8
  40.0 1.1 fusion.38
  41.0 1.3 reshape.478
  42.3 2.1 %fusion.77 = (f32[4,4,96]{2,1,0:T(4,128)S(1)}, f32[4,4,96,224]{3,2,1,0:T(8,128)S(1)}) fusion(bf16[224,4,4,64]{3,2,1,0:T(4,128)(2,1)} %reshape.478, bf16[96,4,4,64]{3,2,1,0:T(4,128)(2,1)} %reshape.477, pred[4,96,224]{2,1,0:T(8,128)(4,1)S(1)} %copy-done.15), kind=kOutput, calls=%fused_computation.123 | convolution fusion | flops 45070848 | bytes 2123776 | tf_op jit(solution)/shard_map/jqchx,jkchx->jchqk/dot_general | solution.py:47
  45.2 0.7 reshape.490
  45.9 0.7 reshape.498
  46.8 0.7 reshape.479
  47.6 0.7 reshape.493
  48.3 1.0 fusion.37
  49.3 1.3 reshape.485
  50.6 1.9 %collective-permute-start.2 = (bf16[384,256]{1,0:T(8,128)(2,1)}, bf16[384,256]{1,0:T(8,128)(2,1)}, u32[]{:S(2)}, u32[]{:S(2)}) collective-permute-start(bf16[384,256]{1,0:T(8,128)(2,1)} %copy-done.10), channel_id=1, source_target_pairs={{0,4},{4,8},{8,12},{1,5},{5,9},{9,13},{2,6},{6,10},{10,14},{3,7},{... | collective-permute-start | bytes 589832 | tf_op jit(solution)/shard_map/ppermute | solution.py:23
  52.5 1.9 %convolution_bitcast_fusion = f32[1,96,4,4,64]{1,4,3,2,0:T(8,128)S(1)} fusion(bf16[224,4,4,64]{3,2,1,0:T(4,128)(2,1)} %reshape.485, f32[4,4,96,224]{3,2,1,0:T(8,128)S(1)} %get-tuple-element.22, f32[4,4,96]{2,1,0:T(4,128)S(1)} %get-tuple-element.21), kind=kOutput, calls=%fused_computation.22 | convolution fusion | flops 44728320 | bytes 2234368 | tf_op jit(solution)/shard_map/jchqk,jkchx->jqchx/dot_general | solution.py:70
  55.2 1.0 copy.134
  56.2 1.2 reshape.486
  57.4 2.0 %copy.122 = f32[384,256]{0,1:T(8,128)} copy(f32[384,256]{1,0:T(8,128)} %reshape.486) | data formatting | bytes 786432 | tf_op jit(solution)/shard_map/reshape | solution.py:76
  59.4 2.1 %collective-permute-start.5 = (bf16[384,256]{1,0:T(8,128)(2,1)}, bf16[384,256]{1,0:T(8,128)(2,1)S(1)}, u32[]{:S(2)}, u32[]{:S(2)}) collective-permute-start(bf16[384,256]{1,0:T(8,128)(2,1)} %collective-permute-done.4), channel_id=1, source_target_pairs={{0,4},{4,8},{8,12},{1,5},{5,9},{9,13},{2,6},{6,10},{10,14},{3,7},{... | collective-permute-start | bytes 589832 | tf_op jit(solution)/shard_map/ppermute | solution.py:23
  61.5 0.9 constant_dynamic-update-slice_fusion.3
  62.5 0.9 constant_dynamic-update-slice_fusion.2
  63.4 0.9 constant_dynamic-update-slice_fusion.1
  64.4 2.0 %reshape.481 = bf16[152,16,4,64]{3,2,1,0:T(4,128)(2,1)} reshape(bf16[2432,256]{1,0:T(8,128)(2,1)S(1)} %constant_dynamic-update-slice_fusion) | data formatting | bytes 2490368 | tf_op jit(solution)/shard_map/reshape.38
  66.4 4.2 %fusion.76 = (f32[16,4,24]{2,1,0:T(4,128)S(1)}, f32[16,4,24,152]{3,2,1,0:T(8,128)S(1)}) fusion(bf16[152,16,4,64]{3,2,1,0:T(4,128)(2,1)} %reshape.481, bf16[24,16,4,64]{3,2,1,0:T(4,128)(2,1)S(1)} %copy-done.11, pred[16,24,152]{2,1,0:T(8,128)(4,1)S(1)} %copy-done.14), kind=kOutput, calls=%fused_computation.122 | convolution fusion | flops 30583296 | bytes 2440192 | tf_op jit(solution)/shard_map/jqchx,jkchx->jchqk/dot_general | solution.py:47
  70.7 1.1 copy-done.1
  72.5 0.7 reshape.491
  73.2 0.7 reshape.499
  74.0 0.7 reshape.482
  74.7 0.7 reshape.494
  75.3 0.7 constant_dynamic-update-slice_fusion.7
  76.0 1.6 %constant_dynamic-update-slice_fusion.6 = bf16[2432,256]{1,0:T(8,128)(2,1)} fusion(bf16[2432,256]{1,0:T(8,128)(2,1)} %constant_dynamic-update-slice_fusion.7, bf16[384,256]{1,0:T(8,128)(2,1)} %collective-permute-done.4), kind=kLoop, calls=%fused_computation.87 | loop fusion | bytes 393216
  77.7 0.7 constant_dynamic-update-slice_fusion.5
  78.4 0.7 constant_dynamic-update-slice_fusion.4
  79.1 3.7 %reshape.487 = bf16[152,16,4,64]{3,2,1,0:T(4,128)(2,1)S(1)} reshape(bf16[2432,256]{1,0:T(8,128)(2,1)} %constant_dynamic-update-slice_fusion.4) | data formatting | bytes 2490368 | tf_op jit(solution)/shard_map/reshape.55
  82.8 3.7 %fusion.14 = f32[1,24,16,4,64]{4,1,3,2,0:T(8,128)S(1)} fusion(bf16[152,16,4,64]{3,2,1,0:T(4,128)(2,1)S(1)} %reshape.487, f32[16,4,24,152]{3,2,1,0:T(8,128)} %copy-done.1, f32[16,4,24]{2,1,0:T(4,128)} %copy-done.12), kind=kOutput, calls=%fused_computation.21 | convolution fusion | flops 30351360 | bytes 2578432 | tf_op jit(solution)/shard_map/jchqk,jkchx->jqchx/dot_general | solution.py:70
  87.2 1.2 reshape.488
  88.4 2.0 %copy.125 = f32[384,256]{0,1:T(8,128)} copy(f32[384,256]{1,0:T(8,128)} %reshape.488) | data formatting | bytes 786432 | tf_op jit(solution)/shard_map/reshape | solution.py:76
  90.5 1.0 copy.137
  91.5 0.8 fusion.65
  92.3 1.8 %multiply_reduce_fusion = (f32[3,128]{1,0:T(4,128)S(1)}, f32[3,128,1,4,64]{1,4,3,0,2:T(8,128)S(1)}) fusion(f32[3,128,1,4,64]{1,4,3,0,2:T(8,128)} %copy.137, f32[3,128,1,4,64]{1,4,3,0,2:T(8,128)} %copy.134, f32[3,128,4]{1,2,0:T(4,128)S(1)} %get-tuple-element.5, f32[3,128,4]{1,2,0:T(4,128)S(1)} %get-tuple-element.7, f32[3,128,4]{1,2,0:T(4,128)S(1)} %get-tuple-element.6, ...), kind=kOutput, calls=%fused_computation.60 | convolution fusion | flops 52297344 | bytes 3177984 | tf_op jit(solution)/shard_map/jchqk,jkchx->jqchx/dot_general | solution.py:70
  94.7 1.8 %convolution_convert_fusion = bf16[384,2048]{1,0:T(8,128)(2,1)} fusion(bf16[384,256]{0,1:T(8,128)(2,1)S(1)} %fusion.54, bf16[256,2048]{1,0:T(8,128)(2,1)S(1)} %copy-done), kind=kOutput, calls=%fused_computation.4 | convolution fusion | flops 403439616 | bytes 2818048 | tf_op jit(solution)/shard_map/dot_general | solution.py:157
  96.5 7.0 %psum.7 = f32[384]{0:T(512)S(1)} all-reduce(f32[384]{0:T(512)S(1)} %bitcast.195), channel_id=1, replica_groups=mesh['grp'=2,'sp'=4,'tp'=4] {'tp'}, use_global_device_ids=true, to_apply=%region_9.10 | all-reduce | flops 384 | bytes 3072 | tf_op jit(solution)/shard_map/psum | solution.py:152
  103.5 22.0 %reduce-scatter.2.cloned.1.call-done = bf16[96,2048]{1,0:T(8,128)(2,1)} async-done(((bf16[384,2048]{1,0:T(8,128)(2,1)}), bf16[96,2048]{1,0:T(8,128)(2,1)}) %reduce-scatter.2.cloned.1.call-update) | async-done | bytes 393232 | tf_op jit(solution)/shard_map/reduce_scatter | solution.py:156
  125.5 1.9 %multiply_convert_fusion = bf16[96,2048]{1,0:T(8,128)(2,1)} fusion(bf16[96,2048]{1,0:T(8,128)(2,1)} %reduce-scatter.2.cloned.1.call-done, f32[96]{0:T(128)S(1)} %dynamic_slice.3), kind=kLoop, calls=%fused_computation.32 | loop fusion | flops 589824 | bytes 786816 | tf_op jit(solution)/shard_map/convert_element_type | solution.py:165
  (90 shorter events, 5.3 us)
Async XLA Ops:
  6.5 88.1 %copy-start = (bf16[256,2048]{1,0:T(8,128)(2,1)S(1)}, bf16[256,2048]{1,0:T(8,128)(2,1)}, u32[]{:S(2)}) copy-start(bf16[256,2048]{1,0:T(8,128)(2,1)} %param.13) | copy-start | bytes 3145732
  6.5 2.0 %copy-start.3 = (bf16[384,2048]{1,0:T(8,128)(2,1)S(1)}, bf16[384,2048]{1,0:T(8,128)(2,1)}, u32[]{:S(2)}) copy-start(bf16[384,2048]{1,0:T(8,128)(2,1)} %param.7) | copy-start | bytes 4718596
  6.5 119.0 %reduce-scatter.2.cloned.1.call-start = ((), (), s32[]{:S(2)}) async-start(), calls=%async_computation.1 | async-start | bytes 1966080 | tf_op jit(solution)/shard_map/reduce_scatter | solution.py:156
  8.5 5.3 %copy-start.22 = (bf16[2048,256]{1,0:T(8,128)(2,1)S(1)}, bf16[2048,256]{1,0:T(8,128)(2,1)}, u32[]{:S(2)}) copy-start(bf16[2048,256]{1,0:T(8,128)(2,1)} %param.10) | copy-start | bytes 3145732
  8.5 5.3 %copy-start.24 = (f32[2048]{0:T(1024)S(1)}, f32[2048]{0:T(1024)}, u32[]{:S(2)}) copy-start(f32[2048]{0:T(1024)} %param.8) | copy-start | bytes 24580
  10.4 7.2 %copy-start.23 = (bf16[2048,256]{1,0:T(8,128)(2,1)S(1)}, bf16[2048,256]{1,0:T(8,128)(2,1)}, u32[]{:S(2)}) copy-start(bf16[2048,256]{1,0:T(8,128)(2,1)} %param.9) | copy-start | bytes 3145732
  10.4 21.5 %collective-permute-start.3 = (bf16[384,256]{1,0:T(8,128)(2,1)S(1)}, bf16[384,256]{1,0:T(8,128)(2,1)S(1)}, u32[]{:S(2)}, u32[]{:S(2)}) collective-permute-start(bf16[384,256]{1,0:T(8,128)(2,1)S(1)} %fusion.26), channel_id=1, source_target_pairs={{0,4},{4,8},{8,12},{1,5},{5,9},{9,13},{2,6},{6,10},{10,14},{3,7},{... | collective-permute-start | bytes 589832 | tf_op jit(solution)/shard_map/ppermute | solution.py:23
  14.4 10.9 %collective-permute-start = (bf16[384,256]{1,0:T(8,128)(2,1)S(1)}, bf16[384,256]{1,0:T(8,128)(2,1)}, u32[]{:S(2)}, u32[]{:S(2)}) collective-permute-start(bf16[384,256]{1,0:T(8,128)(2,1)S(1)} %fusion.23), channel_id=1, source_target_pairs={{0,4},{4,8},{8,12},{1,5},{5,9},{9,13},{2,6},{6,10},{10,14},{3,7},{... | collective-permute-start | bytes 589832 | tf_op jit(solution)/shard_map/ppermute | solution.py:23
  28.4 11.5 %collective-permute-start.1 = (bf16[384,256]{1,0:T(8,128)(2,1)}, bf16[384,256]{1,0:T(8,128)(2,1)S(1)}, u32[]{:S(2)}, u32[]{:S(2)}) collective-permute-start(bf16[384,256]{1,0:T(8,128)(2,1)} %collective-permute-done), channel_id=1, source_target_pairs={{0,4},{4,8},{8,12},{1,5},{5,9},{9,13},{2,6},{6,10},{10,14},{3,7},{... | collective-permute-start | bytes 589832 | tf_op jit(solution)/shard_map/ppermute | solution.py:23
  32.0 8.0 %copy-start.4 = (f32[3,4,128,256]{3,2,1,0:T(8,128)}, f32[3,4,128,256]{3,2,1,0:T(8,128)S(1)}, u32[]{:S(2)}) copy-start(f32[3,4,128,256]{3,2,1,0:T(8,128)S(1)} %get-tuple-element.24) | copy-start | bytes 4718596
  32.0 8.0 %copy-start.8 = (bf16[384,256]{1,0:T(8,128)(2,1)}, bf16[384,256]{1,0:T(8,128)(2,1)S(1)}, u32[]{:S(2)}) copy-start(bf16[384,256]{1,0:T(8,128)(2,1)S(1)} %collective-permute-done.3) | copy-start | bytes 589828
  36.9 11.4 %collective-permute-start.4 = (bf16[384,256]{1,0:T(8,128)(2,1)S(1)}, bf16[384,256]{1,0:T(8,128)(2,1)}, u32[]{:S(2)}, u32[]{:S(2)}) collective-permute-start(bf16[384,256]{1,0:T(8,128)(2,1)S(1)} %collective-permute-done.3), channel_id=1, source_target_pairs={{0,4},{4,8},{8,12},{1,5},{5,9},{9,13},{2,6},{6,10},{10,14},{3,7},{... | collective-permute-start | bytes 589832 | tf_op jit(solution)/shard_map/ppermute | solution.py:23
  39.9 2.4 %copy-start.15 = (pred[4,96,224]{2,1,0:T(8,128)(4,1)S(1)}, pred[4,96,224]{2,1,0:T(8,128)(4,1)}, u32[]{:S(2)}) copy-start(pred[4,96,224]{2,1,0:T(8,128)(4,1)} %broadcast_and_fusion.1) | copy-start | bytes 258052
  40.0 4.5 %copy-start.10 = (bf16[384,256]{1,0:T(8,128)(2,1)}, bf16[384,256]{1,0:T(8,128)(2,1)S(1)}, u32[]{:S(2)}) copy-start(bf16[384,256]{1,0:T(8,128)(2,1)S(1)} %collective-permute-done.1) | copy-start | bytes 589828
  50.6 10.9 %collective-permute-start.2 = (bf16[384,256]{1,0:T(8,128)(2,1)}, bf16[384,256]{1,0:T(8,128)(2,1)}, u32[]{:S(2)}, u32[]{:S(2)}) collective-permute-start(bf16[384,256]{1,0:T(8,128)(2,1)} %copy-done.10), channel_id=1, source_target_pairs={{0,4},{4,8},{8,12},{1,5},{5,9},{9,13},{2,6},{6,10},{10,14},{3,7},{... | collective-permute-start | bytes 589832 | tf_op jit(solution)/shard_map/ppermute | solution.py:23
  56.2 5.3 %copy-start.2 = (bf16[2432,256]{1,0:T(8,128)(2,1)S(1)}, bf16[2432,256]{1,0:T(8,128)(2,1)}, u32[]{:S(2)}) copy-start(bf16[2432,256]{1,0:T(8,128)(2,1)} %broadcast_dynamic-update-slice_fusion.1) | copy-start | bytes 3735556
  59.4 15.9 %collective-permute-start.5 = (bf16[384,256]{1,0:T(8,128)(2,1)}, bf16[384,256]{1,0:T(8,128)(2,1)S(1)}, u32[]{:S(2)}, u32[]{:S(2)}) collective-permute-start(bf16[384,256]{1,0:T(8,128)(2,1)} %collective-permute-done.4), channel_id=1, source_target_pairs={{0,4},{4,8},{8,12},{1,5},{5,9},{9,13},{2,6},{6,10},{10,14},{3,7},{... | collective-permute-start | bytes 589832 | tf_op jit(solution)/shard_map/ppermute | solution.py:23
  64.4 2.0 %copy-start.11 = (bf16[24,16,4,64]{3,2,1,0:T(4,128)(2,1)S(1)}, bf16[24,16,4,64]{3,2,1,0:T(4,128)(2,1)}, u32[]{:S(2)}) copy-start(bf16[24,16,4,64]{3,2,1,0:T(4,128)(2,1)} %reshape.480) | copy-start | bytes 589828
  64.4 2.0 %copy-start.14 = (pred[16,24,152]{2,1,0:T(8,128)(4,1)S(1)}, pred[16,24,152]{2,1,0:T(8,128)(4,1)}, u32[]{:S(2)}) copy-start(pred[16,24,152]{2,1,0:T(8,128)(4,1)} %broadcast_and_fusion) | copy-start | bytes 175108
  70.7 1.2 copy-start.1
  70.7 7.7 %copy-start.12 = (f32[16,4,24]{2,1,0:T(4,128)}, f32[16,4,24]{2,1,0:T(4,128)S(1)}, u32[]{:S(2)}) copy-start(f32[16,4,24]{2,1,0:T(4,128)S(1)} %get-tuple-element.19) | copy-start | bytes 18436
  70.7 7.0 %copy-start.9 = (bf16[384,256]{1,0:T(8,128)(2,1)S(1)}, bf16[384,256]{1,0:T(8,128)(2,1)}, u32[]{:S(2)}) copy-start(bf16[384,256]{1,0:T(8,128)(2,1)} %copy-done.8) | copy-start | bytes 589828
  87.2 4.3 %copy-start.16 = (f32[3,4,128]{2,1,0:T(4,128)S(1)}, f32[3,4,128]{2,1,0:T(4,128)}, u32[]{:S(2)}) copy-start(f32[3,4,128]{2,1,0:T(4,128)} %fusion.8) | copy-start | bytes 18436
  87.2 5.0 %copy-start.13 = (bf16[256,256]{0,1:T(8,128)(2,1)S(1)}, bf16[256,256]{0,1:T(8,128)(2,1)}, u32[]{:S(2)}) copy-start(bf16[256,256]{0,1:T(8,128)(2,1)} %copy.113) | copy-start | bytes 393220
  88.4 3.8 %copy-start.5 = (f32[3,4,128,256]{3,2,1,0:T(8,128)S(1)}, f32[3,4,128,256]{3,2,1,0:T(8,128)}, u32[]{:S(2)}) copy-start(f32[3,4,128,256]{3,2,1,0:T(8,128)} %copy-done.4) | copy-start | bytes 4718596
  92.2 2.2 %copy-start.17 = (f32[384,4]{0,1:T(4,128)S(1)}, f32[384,4]{0,1:T(4,128)}, u32[]{:S(2)}) copy-start(f32[384,4]{0,1:T(4,128)} %reshape.490) | copy-start | bytes 18436
  92.3 2.2 %copy-start.18 = (f32[384,4]{0,1:T(4,128)S(1)}, f32[384,4]{0,1:T(4,128)}, u32[]{:S(2)}) copy-start(f32[384,4]{0,1:T(4,128)} %reshape.479) | copy-start | bytes 18436
  92.3 2.2 %copy-start.19 = (f32[384,4]{0,1:T(4,128)S(1)}, f32[384,4]{0,1:T(4,128)}, u32[]{:S(2)}) copy-start(f32[384,4]{0,1:T(4,128)} %reshape.491) | copy-start | bytes 18436
  92.3 2.2 %copy-start.20 = (f32[384,4]{0,1:T(4,128)S(1)}, f32[384,4]{0,1:T(4,128)}, u32[]{:S(2)}) copy-start(f32[384,4]{0,1:T(4,128)} %reshape.482) | copy-start | bytes 18436
  92.3 2.2 %copy-start.6 = (f32[384,256]{0,1:T(8,128)S(1)}, f32[384,256]{0,1:T(8,128)}, u32[]{:S(2)}) copy-start(f32[384,256]{0,1:T(8,128)} %copy.122) | copy-start | bytes 1179652
  92.3 2.2 %copy-start.7 = (f32[384,256]{0,1:T(8,128)S(1)}, f32[384,256]{0,1:T(8,128)}, u32[]{:S(2)}) copy-start(f32[384,256]{0,1:T(8,128)} %copy.125) | copy-start | bytes 1179652
  92.3 2.2 %copy-start.21 = (f32[256]{0:T(256)S(1)}, f32[256]{0:T(256)}, u32[]{:S(2)}) copy-start(f32[256]{0:T(256)} %param.12) | copy-start | bytes 3076
Sparse Core Ops, SparseCore 0:
  96.6 28.8 reduce-scatter.1
where the time goes:
time: 137 us; the launch traced here: 134 us
  local copies, waits for them, and re-layouts  44.4 us (32%)
  waiting for transfers between devices  22 us (16%)
  matrix products  20.2 us (15%)
  starting transfers between devices  14.4 us (11%)
  between operations  14 us (10%)
  other arithmetic  12.3 us (9%)
  blocking collectives  6.98 us (5%)
    reduce_scatter x1, waiting for transfers between devices, on_device(): lax.psum_scatter(jnp.dot(gated, w_out, preferred_element_type=jnp.float32...  22 us
    ppermute x6, starting transfers between devices, from_behind(): lax.ppermute(value, axis, [(source, source + steps) for source in range(i...  14.4 us
    another operation x7, local copies, waits for them, and re-layouts  11.3 us
    unnamed x58, local copies, waits for them, and re-layouts  8.73 us
    reshape x6, local copies, waits for them, and re-layouts, band_part(): weighted = weighted.reshape(query_len, head_count, head_width)  8.44 us
    dot_general x3, matrix products, band_part(): jnp.einsum('jqchx,jkchx->jchqk', query_blk, key_blk, preferred_element_ty...  7.97 us
    dot_general x3, matrix products, band_part(): jnp.einsum('jchqk,jkchx->jqchx', weights.astype(jnp.bfloat16), value_blk,...  7.39 us
    psum x1, blocking collectives, on_device(): squares = lax.psum(jnp.sum(attended * attended, axis=-1), 'tp')  6.98 us
  transfers between devices with their start and end apart: 7, of which 1 were waited for; matrix products, arithmetic and copies ran while one was open for 35% of the time, Pallas kernels for 0%

commit v1 on v0

v1 whole, which is shorter than its diff:
```python
import functools
import math

import jax
import jax.numpy as jnp
from jax import lax
from jax.experimental import pallas as pl
from jax.experimental.pallas import tpu as pltpu
from jax.sharding import PartitionSpec as P

HEAD_DIM = 64
PATTERNS = ((128, 1), (512, 4), (2048, 16))
REACH = max(window for window, _ in PATTERNS)
EPS = 1e-06
NEG = -1e30
MESH = pl.DeviceIdType.MESH
ROW_BLOCK = 128
HALVES = 2


def log_multiplicity(rows, cols, first_lag):
    low, high = first_lag - (cols - 1), first_lag + rows - 1
    lag = (
        first_lag
        + lax.broadcasted_iota(jnp.int32, (rows, cols), 0)
        - lax.broadcasted_iota(jnp.int32, (rows, cols), 1)
    )
    count = jnp.zeros((rows, cols), jnp.int32)
    for window, dilation in PATTERNS:
        if high < 0 or low > window:
            continue
        reads = (lag & (dilation - 1)) == 0
        if low < 0:
            reads = reads & (lag >= 0)
        if high > window:
            reads = reads & (lag <= window)
        count = count + reads.astype(jnp.int32)
    return jnp.where(
        count == 0,
        NEG,
        jnp.where(count == 1, 0.0, jnp.where(count == 2, 1.0, math.log2(3.0))),
    )


def kernel(
    n_sp,
    n_tp,
    reach,
    tok_hbm,
    gain_ref,
    wq_hbm,
    wk_hbm,
    wv_hbm,
    og_hbm,
    wo_hbm,
    out_ref,
    tok,
    scaled,
    wq,
    wk,
    wv,
    og,
    wo,
    query,
    keys,
    values,
    top,
    total,
    partial,
    att,
    got,
    load_sem,
    k_send,
    k_recv,
    v_send,
    v_recv,
    wo_send,
    wo_recv,
    wo_fsend,
    og_send,
    og_recv,
    att_send,
    att_recv,
):
    z = lax.axis_index("sp")
    me = lax.axis_index("tp")
    rows, channels = query.shape
    heads = channels // HEAD_DIM
    share = rows // n_tp
    chips = n_tp // 2
    chip, core = me // 2, lax.rem(me, 2)
    sibling = chip * 2 + 1 - core
    has_next = z + 1 < n_sp

    loads = [
        pltpu.make_async_copy(source, target, load_sem.at[number])
        for number, (source, target) in enumerate(
            ((tok_hbm, tok), (wk_hbm, wk), (wv_hbm, wv), (wq_hbm, wq), (og_hbm, og.at[me]), (wo_hbm, wo.at[me]))
        )
    ]
    for load in loads:
        load.start()

    barrier = pltpu.get_barrier_semaphore()
    for step in range(1, n_tp):
        pl.semaphore_signal(
            barrier, inc=1, device_id={"tp": lax.rem(me + step, n_tp)}, device_id_type=MESH
        )

    @pl.when(z > 0)
    def _():
        pl.semaphore_signal(barrier, inc=1, device_id={"sp": z - 1}, device_id_type=MESH)

    @pl.when(has_next)
    def _():
        pl.semaphore_signal(barrier, inc=1, device_id={"sp": z + 1}, device_id_type=MESH)

    neighbours = (z > 0).astype(jnp.int32) + has_next.astype(jnp.int32)
    pl.semaphore_wait(barrier, n_tp - 1 + neighbours)

    half = channels // HALVES

    def part_of(piece):
        return pl.ds(piece * half, half)

    def wo_copy(slot, piece, target):
        return pltpu.make_async_remote_copy(
            src_ref=wo_hbm.at[part_of(piece)],
            dst_ref=wo.at[me, part_of(piece)],
            send_sem=wo_send.at[slot, piece],
            recv_sem=wo_recv.at[me, piece],
            device_id={"tp": target},
            device_id_type=MESH,
        )

    wo_targets = [lax.rem(chip + step, chips) * 2 + core for step in range(1, chips)] + [sibling]
    wo_sends = [
        wo_copy(slot, piece, target)
        for piece in range(HALVES)
        for slot, target in enumerate(wo_targets)
    ]
    for copy in wo_sends:
        copy.start()

    def wo_arrived(shard, piece):
        pltpu.make_async_remote_copy(
            src_ref=wo.at[shard, part_of(piece)],
            dst_ref=wo.at[shard, part_of(piece)],
            send_sem=wo_send.at[0, piece],
            recv_sem=wo_recv.at[shard, piece],
            device_id={"tp": sibling},
            device_id_type=MESH,
        ).wait_recv()

    def forward(step, piece):
        shard = lax.rem(chip + step, chips) * 2 + core
        return pltpu.make_async_remote_copy(
            src_ref=wo.at[shard, part_of(piece)],
            dst_ref=wo.at[shard, part_of(piece)],
            send_sem=wo_fsend.at[step, piece],
            recv_sem=wo_recv.at[shard, piece],
            device_id={"tp": sibling},
            device_id_type=MESH,
        )

    def forward_piece(piece):
        for step in range(1, chips):
            wo_arrived(lax.rem(chip + step, chips) * 2 + core, piece)
            forward(step, piece).start()

    og_sends = [
        pltpu.make_async_remote_copy(
            src_ref=og_hbm,
            dst_ref=og.at[me],
            send_sem=og_send.at[step],
            recv_sem=og_recv.at[me],
            device_id={"tp": lax.rem(me + step, n_tp)},
            device_id_type=MESH,
        )
        for step in range(1, n_tp)
    ]
    for copy in og_sends:
        copy.start()

    def relay(buffer, send, recv, distance):
        return pltpu.make_async_remote_copy(
            src_ref=buffer.at[distance],
            dst_ref=buffer.at[distance + 1],
            send_sem=send.at[distance],
            recv_sem=recv.at[distance + 1],
            device_id={"sp": z + 1},
            device_id_type=MESH,
        )

    def arrived(buffer, send, recv, distance):
        pltpu.make_async_remote_copy(
            src_ref=buffer.at[distance],
            dst_ref=buffer.at[distance],
            send_sem=send.at[0],
            recv_sem=recv.at[distance],
            device_id={"sp": z - 1},
            device_id_type=MESH,
        ).wait_recv()

    loads[0].wait()
    wide = tok[...].astype(jnp.float32)
    inverse = lax.rsqrt(jnp.mean(wide * wide, axis=-1, keepdims=True) + EPS)
    scaled[...] = (wide * gain_ref[...]).astype(jnp.bfloat16)

    def project(weight):
        product = jnp.dot(scaled[...], weight[...], preferred_element_type=jnp.float32)
        return (product * inverse).astype(jnp.bfloat16)

    loads[1].wait()
    keys[0] = project(wk)

    @pl.when(has_next)
    def _():
        relay(keys, k_send, k_recv, 0).start()

    loads[2].wait()
    values[0] = project(wv)

    @pl.when(has_next)
    def _():
        relay(values, v_send, v_recv, 0).start()

    loads[3].wait()
    query[...] = project(wq)

    lane_head = lax.broadcasted_iota(jnp.int32, (ROW_BLOCK, channels), 1) // HEAD_DIM
    factor = HEAD_DIM ** (-0.5) * math.log2(math.e)

    def attend(distance):
        for first in range(0, rows, ROW_BLOCK):
            cols = min(rows, first + ROW_BLOCK) if distance == 0 else rows
            first_lag = first + distance * rows
            if first_lag - (cols - 1) > REACH:
                continue
            block = pl.ds(first, ROW_BLOCK)
            bias = log_multiplicity(ROW_BLOCK, cols, first_lag)
            q_rows = query[block, :]
            key_rows = keys[distance, :cols, :]
            value_rows = values[distance, :cols, :]
            mixed, scale = None, None
            for head in range(heads):
                q_head = jnp.where(lane_head == head, q_rows, jnp.zeros_like(q_rows))
                scores = lax.dot_general(
                    q_head, key_rows, (((1,), (1,)), ((), ())), preferred_element_type=jnp.float32
                )
                scores = scores * factor + bias
                peak = jnp.max(scores, axis=-1, keepdims=True)
                if distance:
                    old = top[head, block, :]
                    peak = jnp.maximum(peak, old)
                    shrink = jnp.exp2(old - peak)
                weights = jnp.exp2(scores - peak)
                sums = jnp.sum(weights, axis=-1, keepdims=True)
                if distance:
                    sums = sums + shrink * total[head, block, :]
                    wide_shrink = jnp.broadcast_to(shrink, (ROW_BLOCK, channels))
                    scale = wide_shrink if scale is None else jnp.where(lane_head == head, wide_shrink, scale)
                top[head, block, :] = peak
                total[head, block, :] = sums
                product = jnp.dot(
                    weights.astype(jnp.bfloat16), value_rows, preferred_element_type=jnp.float32
                )
                mixed = product if mixed is None else jnp.where(lane_head == head, product, mixed)
            if distance:
                mixed = mixed + scale * partial[block, :]
            partial[block, :] = mixed

    attend(0)
    forwarded = 0
    for distance in range(1, reach + 1):

        @pl.when(z >= distance)
        def _():
            arrived(keys, k_send, k_recv, distance)
            if distance < reach:

                @pl.when(has_next)
                def _():
                    relay(keys, k_send, k_recv, distance).start()

            arrived(values, v_send, v_recv, distance)
            if distance < reach:

                @pl.when(has_next)
                def _():
                    relay(values, v_send, v_recv, distance).start()

            attend(distance)

        if forwarded < HALVES - 1 and distance >= 2:
            forward_piece(forwarded)
            forwarded += 1
    for piece in range(forwarded, HALVES):
        forward_piece(piece)

    def att_copy(step):
        target = lax.rem(me + step, n_tp)
        return pltpu.make_async_remote_copy(
            src_ref=att.at[target],
            dst_ref=got.at[me],
            send_sem=att_send.at[step],
            recv_sem=att_recv.at[me],
            device_id={"tp": target},
            device_id_type=MESH,
        )

    spread_head = lax.broadcasted_iota(jnp.int32, (share, channels), 1) // HEAD_DIM
    for part in range(n_tp):
        piece = pl.ds(part * share, share)
        denominator = jnp.broadcast_to(total[0, piece, :], (share, channels))
        for head in range(1, heads):
            denominator = jnp.where(
                spread_head == head,
                jnp.broadcast_to(total[head, piece, :], (share, channels)),
                denominator,
            )
        att[part] = (partial[piece, :] / denominator).astype(jnp.bfloat16)
    att_sends = [att_copy(step) for step in range(1, n_tp)]
    for copy in att_sends:
        copy.start()

    loads[4].wait()
    loads[5].wait()
    for step in range(1, n_tp):
        peer = lax.rem(me + step, n_tp)
        pltpu.make_async_remote_copy(
            src_ref=og_hbm,
            dst_ref=og.at[peer],
            send_sem=og_send.at[step],
            recv_sem=og_recv.at[peer],
            device_id={"tp": peer},
            device_id_type=MESH,
        ).wait_recv()
    for piece in range(HALVES):
        wo_arrived(sibling, piece)
        for step in range(1, chips):
            wo_arrived(lax.rem(chip + step, chips) * 2 + 1 - core, piece)

    def norm_and_gate(rows_of, gain_of):
        row_values = rows_of.astype(jnp.float32)
        return (
            jnp.sum(row_values * row_values, axis=-1, keepdims=True),
            (row_values * gain_of).astype(jnp.bfloat16),
        )

    squares, gated = norm_and_gate(att[me], og[me])
    summed = jnp.dot(gated, wo[me], preferred_element_type=jnp.float32)
    for step in range(1, n_tp):
        peer = lax.rem(me + step, n_tp)
        pltpu.make_async_remote_copy(
            src_ref=att.at[peer],
            dst_ref=got.at[peer],
            send_sem=att_send.at[step],
            recv_sem=att_recv.at[peer],
            device_id={"tp": peer},
            device_id_type=MESH,
        ).wait_recv()
        more, gated = norm_and_gate(got[peer], og[peer])
        squares = squares + more
        summed = summed + jnp.dot(gated, wo[peer], preferred_element_type=jnp.float32)
    norm = lax.rsqrt(squares / (channels * n_tp) + EPS)
    out_ref[...] = (summed * norm).astype(jnp.bfloat16)

    for copy in wo_sends + og_sends + att_sends:
        copy.wait_send()
    for piece in range(HALVES):
        for step in range(1, chips):
            forward(step, piece).wait_send()
    for distance in range(reach):

        @pl.when(has_next & (z >= distance))
        def _():
            relay(keys, k_send, k_recv, distance).wait_send()
            relay(values, v_send, v_recv, distance).wait_send()


def on_device(n_sp, n_tp, tokens, norm_gain, w_query, w_key, w_value, out_gain, w_out):
    rows, width = tokens.shape
    channels = w_query.shape[1]
    heads = channels // HEAD_DIM
    share = rows // n_tp
    reach = min(-(-REACH // rows), n_sp - 1)
    hbm = pl.BlockSpec(memory_space=pl.ANY)
    vmem = pl.BlockSpec(memory_space=pltpu.VMEM)
    dma = pltpu.SemaphoreType.DMA
    bf16, f32 = jnp.bfloat16, jnp.float32
    return pl.pallas_call(
        functools.partial(kernel, n_sp, n_tp, reach),
        out_shape=jax.ShapeDtypeStruct((share, w_out.shape[1]), bf16),
        in_specs=[hbm, vmem, hbm, hbm, hbm, hbm, hbm],
        out_specs=vmem,
        scratch_shapes=[
            pltpu.VMEM((rows, width), bf16),
            pltpu.VMEM((rows, width), bf16),
            pltpu.VMEM((width, channels), bf16),
            pltpu.VMEM((width, channels), bf16),
            pltpu.VMEM((width, channels), bf16),
            pltpu.VMEM((n_tp, 1, channels), f32),
            pltpu.VMEM((n_tp,) + w_out.shape, bf16),
            pltpu.VMEM((rows, channels), bf16),
            pltpu.VMEM((reach + 1, rows, channels), bf16),
            pltpu.VMEM((reach + 1, rows, channels), bf16),
            pltpu.VMEM((heads, rows, 1), f32),
            pltpu.VMEM((heads, rows, 1), f32),
            pltpu.VMEM((rows, channels), f32),
            pltpu.VMEM((n_tp, share, channels), bf16),
            pltpu.VMEM((n_tp, share, channels), bf16),
            dma((6,)),
            dma((reach + 1,)),
            dma((reach + 1,)),
            dma((reach + 1,)),
            dma((reach + 1,)),
            dma((n_tp // 2, HALVES)),
            dma((n_tp, HALVES)),
            dma((n_tp // 2, HALVES)),
            dma((n_tp,)),
            dma((n_tp,)),
            dma((n_tp,)),
            dma((n_tp,)),
        ],
        compiler_params=pltpu.CompilerParams(
            collective_id=0, has_side_effects=True, vmem_limit_bytes=60 * 1024 * 1024
        ),
    )(tokens, norm_gain[None, :], w_query, w_key, w_value, out_gain[None, :], w_out)


def solution(mesh):
    in_specs = (
        P(("grp", "sp"), None),
        P(),
        P(None, "tp"),
        P(None, "tp"),
        P(None, "tp"),
        P("tp"),
        P("tp", None),
    )
    out_specs = P(("grp", "sp", "tp"), None)
    return jax.shard_map(
        functools.partial(on_device, mesh.shape["sp"], mesh.shape["tp"]),
        mesh=mesh,
        in_specs=in_specs,
        out_specs=out_specs,
        check_vma=False,
    )
```

time: 137 us -> 43 us (0.31)
  the two profiles are of different devices: /device:TPU:9 before, /device:TPU:29 now
where the time goes in v1:
time: 43 us; the launch traced here: 42.8 us
  Pallas kernels  41 us (95%)
  local copies, waits for them, and re-layouts  1.77 us (4%)
    pallas_call x1, Pallas kernels, on_device(): pl.pallas_call(functools.partial(kernel, n_sp, n_tp, reach), out_shape=ja...  41 us
    unnamed x1, local copies, waits for them, and re-layouts  1.77 us

profile of v1, /device:TPU:29, one launch (start us, length us, event | category | flops | bytes accessed | tf_op | source)
XLA Modules:
  0.0 42.8 jit_solution(1633295795850414982)
XLA Ops:
  0.0 41.0 %shard_map.73 = bf16[96,2048]{1,0:T(8,128)(2,1)} custom-call(bf16[384,2048]{1,0:T(8,128)(2,1)} %tok_hbm.1, f32[1,2048]{1,0:T(1,128)} %bitcast.2, bf16[2048,256]{1,0:T(8,128)(2,1)} %wq_hbm.1, bf16[2048,256]{1,0:T(8,128)(2,1)} %wk_hbm.1, bf16[2048,256]{1,0:T(8,128)(2,1)} %wv_hbm.1, f32[1,256]{1,0:T(1,128)} %bitcast.3, bf16[256,2048]{1,0:T(8,128)(2,1)} %wo_hbm.1), custom_call_target="tpu_custom_call" | custom-call | tf_op jit(solution)/shard_map/pallas_call | solution.py:392
  41.0 1.8 %copy.9 = bf16[96,2048]{1,0:T(8,128)(2,1)} copy(bf16[96,2048]{1,0:T(8,128)(2,1)} %shard_map.73) | data formatting | bytes 786432

commit v2 on v1

v2 whole, which is shorter than its diff:
```python
import functools
import math

import jax
import jax.numpy as jnp
from jax import lax
from jax.experimental import pallas as pl
from jax.experimental.pallas import tpu as pltpu
from jax.sharding import PartitionSpec as P

HEAD_DIM = 64
PATTERNS = ((128, 1), (512, 4), (2048, 16))
REACH = max(window for window, _ in PATTERNS)
EPS = 1e-06
NEG = -1e30
MESH = pl.DeviceIdType.MESH
ROW_BLOCK = 128
PIECES = 4


def log_multiplicity(rows, cols, first_lag):
    low, high = first_lag - (cols - 1), first_lag + rows - 1
    lag = (
        first_lag
        + lax.broadcasted_iota(jnp.int32, (rows, cols), 0)
        - lax.broadcasted_iota(jnp.int32, (rows, cols), 1)
    )
    count = jnp.zeros((rows, cols), jnp.int32)
    for window, dilation in PATTERNS:
        if high < 0 or low > window:
            continue
        reads = (lag & (dilation - 1)) == 0
        if low < 0:
            reads = reads & (lag >= 0)
        if high > window:
            reads = reads & (lag <= window)
        count = count + reads.astype(jnp.int32)
    return jnp.where(
        count == 0,
        NEG,
        jnp.where(count == 1, 0.0, jnp.where(count == 2, 1.0, math.log2(3.0))),
    )


def kernel(
    n_grp,
    n_sp,
    n_tp,
    reach,
    tok_hbm,
    gain_ref,
    wq_hbm,
    wk_hbm,
    wv_hbm,
    og_hbm,
    wo_hbm,
    out_ref,
    tok,
    scaled,
    wq,
    wk,
    wv,
    og,
    wo,
    query,
    kv,
    guest,
    top,
    total,
    partial,
    help_att,
    help_lse,
    back_att,
    back_lse,
    att,
    got,
    load_sem,
    kv_send,
    kv_recv,
    q_send,
    q_recv,
    help_send,
    back_recv,
    wo_send,
    wo_recv,
    wo_fsend,
    wo_ysend,
    og_send,
    og_recv,
    att_send,
    att_recv,
):
    z = lax.axis_index("sp")
    me = lax.axis_index("tp")
    grp = lax.axis_index("grp")
    rows = query.shape[1]
    lanes = query.shape[2]
    channels = 2 * lanes
    heads = lanes // HEAD_DIM
    share = rows // n_tp
    chips = n_tp // 2
    chip, core = me // 2, lax.rem(me, 2)
    sibling = chip * 2 + 1 - core
    has_next = z + 1 < n_sp
    helped = n_sp == 4 and reach == 3
    paired = n_grp % 2 == 0
    far = grp + 1 - 2 * lax.rem(grp, 2) if paired else grp
    side = lax.rem(grp, 2) if paired else 0

    loads = [
        pltpu.make_async_copy(source, target, load_sem.at[number])
        for number, (source, target) in enumerate(
            ((tok_hbm, tok), (wk_hbm, wk), (wv_hbm, wv), (wq_hbm, wq), (og_hbm, og.at[me]), (wo_hbm, wo.at[me]))
        )
    ]
    for load in loads:
        load.start()

    barrier = pltpu.get_barrier_semaphore()
    for step in range(1, n_tp):
        pl.semaphore_signal(
            barrier, inc=1, device_id={"tp": lax.rem(me + step, n_tp)}, device_id_type=MESH
        )

    if paired:
        pl.semaphore_signal(barrier, inc=1, device_id={"grp": far}, device_id_type=MESH)
    for hop in ((1, 2) if helped else (1,)):
        if hop == 1:
            backward, onward = z > 0, has_next
        else:
            backward, onward = z == 3, z == 1

        @pl.when(backward)
        def _():
            pl.semaphore_signal(barrier, inc=1, device_id={"sp": z - hop}, device_id_type=MESH)

        @pl.when(onward)
        def _():
            pl.semaphore_signal(barrier, inc=1, device_id={"sp": z + hop}, device_id_type=MESH)

    neighbours = (z > 0).astype(jnp.int32) + has_next.astype(jnp.int32)
    if helped:
        neighbours = neighbours + (z == 3).astype(jnp.int32) + (z == 1).astype(jnp.int32)
    pl.semaphore_wait(barrier, n_tp - 1 + int(paired) + neighbours)

    half = channels // PIECES
    own_pieces = PIECES // 2 if paired else PIECES

    def part_of(piece):
        return pl.ds(pl.multiple_of(piece * half, half), half)

    def wo_copy(slot, piece, target):
        return pltpu.make_async_remote_copy(
            src_ref=wo_hbm.at[part_of(piece)],
            dst_ref=wo.at[me, part_of(piece)],
            send_sem=wo_send.at[slot, piece],
            recv_sem=wo_recv.at[me, piece],
            device_id={"tp": target},
            device_id_type=MESH,
        )

    mine = [side * own_pieces + number for number in range(own_pieces)]
    theirs = [(1 - side) * own_pieces + number for number in range(own_pieces)] if paired else []
    across = [lax.rem(chip + step, chips) * 2 + core for step in range(1, chips)]
    wo_sends = [
        wo_copy(slot, piece, target) for piece in mine for slot, target in enumerate(across)
    ] + [wo_copy(chips - 1, piece, sibling) for piece in range(PIECES)]
    for copy in wo_sends:
        copy.start()

    def passed_on(shard, piece, send_sem, device):
        return pltpu.make_async_remote_copy(
            src_ref=wo.at[shard, part_of(piece)],
            dst_ref=wo.at[shard, part_of(piece)],
            send_sem=send_sem,
            recv_sem=wo_recv.at[shard, piece],
            device_id=device,
            device_id_type=MESH,
        )

    def wo_arrived(shard, piece):
        passed_on(shard, piece, wo_send.at[0, piece], {"tp": sibling}).wait_recv()

    forwards = []

    def forward(pieces, over_y):
        for piece in pieces:
            for step in range(1, chips):
                shard = across[step - 1]
                wo_arrived(shard, piece)
                copies = [passed_on(shard, piece, wo_fsend.at[step, piece], {"tp": sibling})]
                if over_y:
                    copies.insert(0, passed_on(shard, piece, wo_ysend.at[step, piece], {"grp": far}))
                for copy in copies:
                    copy.start()
                forwards.extend(copies)

    og_sends = [
        pltpu.make_async_remote_copy(
            src_ref=og_hbm,
            dst_ref=og.at[me],
            send_sem=og_send.at[step],
            recv_sem=og_recv.at[me],
            device_id={"tp": lax.rem(me + step, n_tp)},
            device_id_type=MESH,
        )
        for step in range(1, n_tp)
    ]
    for copy in og_sends:
        copy.start()

    def relay(part, distance):
        return pltpu.make_async_remote_copy(
            src_ref=kv.at[part, distance],
            dst_ref=kv.at[part, distance + 1],
            send_sem=kv_send.at[part, distance],
            recv_sem=kv_recv.at[part, distance + 1],
            device_id={"sp": z + 1},
            device_id_type=MESH,
        )

    def arrived(part, distance):
        pltpu.make_async_remote_copy(
            src_ref=kv.at[part, distance],
            dst_ref=kv.at[part, distance],
            send_sem=kv_send.at[part, 0],
            recv_sem=kv_recv.at[part, distance],
            device_id={"sp": z - 1},
            device_id_type=MESH,
        ).wait_recv()

    def ship(part, slot, target):
        return pltpu.make_async_remote_copy(
            src_ref=query.at[part],
            dst_ref=guest.at[slot],
            send_sem=q_send.at[part],
            recv_sem=q_recv.at[slot],
            device_id={"sp": target},
            device_id_type=MESH,
        )

    def guest_arrived(slot):
        ship(0, slot, z + 1).wait_recv()

    def send_back(slot, part, target):
        return [
            pltpu.make_async_remote_copy(
                src_ref=mine_ref.at[slot],
                dst_ref=their_ref.at[part],
                send_sem=help_send.at[slot, number],
                recv_sem=back_recv.at[part, number],
                device_id={"sp": target},
                device_id_type=MESH,
            )
            for number, (mine_ref, their_ref) in enumerate(((help_att, back_att), (help_lse, back_lse)))
        ]

    loads[0].wait()
    wide = tok[...].astype(jnp.float32)
    inverse = lax.rsqrt(jnp.mean(wide * wide, axis=-1, keepdims=True) + EPS)
    scaled[...] = (wide * gain_ref[...]).astype(jnp.bfloat16)

    def project(weight):
        product = jnp.dot(scaled[...], weight[...], preferred_element_type=jnp.float32)
        return (product * inverse).astype(jnp.bfloat16)

    def by_half(product):
        return product[:, :lanes], product[:, lanes:]

    loads[1].wait()
    kv[0, 0, 0], kv[1, 0, 0] = by_half(project(wk))
    loads[2].wait()
    kv[0, 0, 1], kv[1, 0, 1] = by_half(project(wv))

    @pl.when(has_next)
    def _():
        relay(0, 0).start()

    @pl.when(has_next & (z != 1) if helped else has_next)
    def _():
        relay(1, 0).start()

    loads[3].wait()
    query[0], query[1] = by_half(project(wq))
    if helped:

        @pl.when(z == 2)
        def _():
            ship(1, 0, 1).start()

        @pl.when(z == 3)
        def _():
            ship(1, 1, 1).start()
            ship(0, 1, 2).start()

    lane_head = lax.broadcasted_iota(jnp.int32, (ROW_BLOCK, lanes), 1) // HEAD_DIM
    factor = HEAD_DIM ** (-0.5) * math.log2(math.e)

    def spread(columns):
        result = jnp.broadcast_to(columns[0], (ROW_BLOCK, lanes))
        for head in range(1, heads):
            result = jnp.where(
                lane_head == head, jnp.broadcast_to(columns[head], (ROW_BLOCK, lanes)), result
            )
        return result

    def attend(parts, state_of, queries_of, slot, distance, fresh):
        for first in range(0, rows, ROW_BLOCK):
            cols = min(rows, first + ROW_BLOCK) if distance == 0 else rows
            first_lag = first + distance * rows
            if first_lag - (cols - 1) > REACH:
                continue
            block = pl.ds(first, ROW_BLOCK)
            bias = log_multiplicity(ROW_BLOCK, cols, first_lag)
            for part in parts:
                state = state_of(part)
                q_rows = queries_of(part)[block, :]
                key_rows = kv[part, slot, 0, :cols, :]
                value_rows = kv[part, slot, 1, :cols, :]
                mixed, shrinks = None, []
                for head in range(heads):
                    q_head = jnp.where(lane_head == head, q_rows, jnp.zeros_like(q_rows))
                    scores = lax.dot_general(
                        q_head,
                        key_rows,
                        (((1,), (1,)), ((), ())),
                        preferred_element_type=jnp.float32,
                    )
                    scores = scores * factor + bias
                    peak = jnp.max(scores, axis=-1, keepdims=True)
                    if not fresh:
                        old = top[state, head, block, :]
                        peak = jnp.maximum(peak, old)
                        shrinks.append(jnp.exp2(old - peak))
                    weights = jnp.exp2(scores - peak)
                    sums = jnp.sum(weights, axis=-1, keepdims=True)
                    if not fresh:
                        sums = sums + shrinks[head] * total[state, head, block, :]
                    top[state, head, block, :] = peak
                    total[state, head, block, :] = sums
                    product = jnp.dot(
                        weights.astype(jnp.bfloat16), value_rows, preferred_element_type=jnp.float32
                    )
                    mixed = product if mixed is None else jnp.where(lane_head == head, product, mixed)
                if not fresh:
                    mixed = mixed + spread(shrinks) * partial[state, block, :]
                partial[state, block, :] = mixed

    def own(parts, distance):
        attend(parts, lambda part: part, lambda part: query.at[part], distance, distance, distance == 0)

    def help_out(part, guest_slot, slot, distance, fresh):
        attend(
            [part], lambda _: 2 + guest_slot, lambda _: guest.at[guest_slot], slot, distance, fresh
        )

    def give_back(guest_slot, part, target):
        state = 2 + guest_slot
        lane = lax.broadcasted_iota(jnp.int32, (ROW_BLOCK, 128), 1)
        pick = (
            lax.broadcasted_iota(jnp.int32, (8, 128), 0) == lax.broadcasted_iota(jnp.int32, (8, 128), 1)
        ).astype(jnp.float32)
        for first in range(0, rows, ROW_BLOCK):
            block = pl.ds(first, ROW_BLOCK)
            sums = [total[state, head, block, :] for head in range(heads)]
            help_att[guest_slot, block, :] = (partial[state, block, :] / spread(sums)).astype(jnp.bfloat16)
            logs = jnp.zeros((ROW_BLOCK, 128), jnp.float32)
            for head in range(heads):
                column = top[state, head, block, :] + jnp.log2(sums[head])
                logs = jnp.where(lane == head, jnp.broadcast_to(column, (ROW_BLOCK, 128)), logs)
            help_lse[guest_slot, :, block] = lax.dot_general(
                pick,
                logs,
                (((1,), (1,)), ((), ())),
                precision=lax.Precision.HIGHEST,
                preferred_element_type=jnp.float32,
            )
        for copy in send_back(guest_slot, part, target):
            copy.start()

    def take_back(part):
        for copy in send_back(0, part, z):
            copy.wait_recv()
        eye = (
            lax.broadcasted_iota(jnp.int32, (ROW_BLOCK, ROW_BLOCK), 0)
            == lax.broadcasted_iota(jnp.int32, (ROW_BLOCK, ROW_BLOCK), 1)
        ).astype(jnp.float32)
        for first in range(0, rows, ROW_BLOCK):
            block = pl.ds(first, ROW_BLOCK)
            logs = lax.dot_general(
                eye,
                back_lse[part, :, block],
                (((1,), (1,)), ((), ())),
                precision=lax.Precision.HIGHEST,
                preferred_element_type=jnp.float32,
            )
            before, after = [], []
            for head in range(heads):
                column, old = logs[:, head : head + 1], top[part, head, block, :]
                peak = jnp.maximum(column, old)
                before.append(jnp.exp2(old - peak))
                after.append(jnp.exp2(column - peak))
                total[part, head, block, :] = total[part, head, block, :] * before[head] + after[head]
            partial[part, block, :] = partial[part, block, :] * spread(before) + back_att[
                part, block, :
            ].astype(jnp.float32) * spread(after)

    both = (0, 1)
    if helped:

        @pl.when(z != 1)
        def _():
            own(both, 0)

        @pl.when(z == 1)
        def _():
            own(both, 0)
            arrived(0, 1)
            relay(0, 1).start()
            guest_arrived(1)
            help_out(1, 1, 0, 2, True)
            guest_arrived(0)
            help_out(1, 0, 0, 1, True)
            own([0], 1)

        forward(mine[:1], paired)

        @pl.when(z == 1)
        def _():
            arrived(1, 1)
            help_out(1, 1, 1, 3, False)
            give_back(1, 1, 3)
            help_out(1, 0, 1, 2, False)
            give_back(0, 1, 2)
            own([1], 1)

        @pl.when(z == 2)
        def _():
            arrived(0, 1)
            guest_arrived(1)
            help_out(0, 1, 1, 2, True)
            own([0], 1)

        forward(mine[1:], paired)

        @pl.when(z == 2)
        def _():
            arrived(0, 2)
            help_out(0, 1, 2, 3, False)
            give_back(1, 0, 3)
            own([0], 2)
            take_back(1)

        @pl.when(z == 3)
        def _():
            arrived(0, 1)
            own([0], 1)
            arrived(1, 1)
            own([1], 1)
            take_back(1)
            take_back(0)

    else:
        own(both, 0)
        for distance in range(1, reach + 1):

            @pl.when(z >= distance)
            def _():
                for part in both:
                    arrived(part, distance)
                    if distance < reach:

                        @pl.when(has_next)
                        def _():
                            relay(part, distance).start()

                own(both, distance)

        forward(mine, paired)

    def att_copy(step):
        target = lax.rem(me + step, n_tp)
        return pltpu.make_async_remote_copy(
            src_ref=att.at[target],
            dst_ref=got.at[me],
            send_sem=att_send.at[step],
            recv_sem=att_recv.at[me],
            device_id={"tp": target},
            device_id_type=MESH,
        )

    spread_head = lax.broadcasted_iota(jnp.int32, (share, lanes), 1) // HEAD_DIM
    for target in range(n_tp):
        piece = pl.ds(target * share, share)
        for part in both:
            denominator = jnp.broadcast_to(total[part, 0, piece, :], (share, lanes))
            for head in range(1, heads):
                denominator = jnp.where(
                    spread_head == head,
                    jnp.broadcast_to(total[part, head, piece, :], (share, lanes)),
                    denominator,
                )
            att[target, :, part * lanes : (part + 1) * lanes] = (
                partial[part, piece, :] / denominator
            ).astype(jnp.bfloat16)
    att_sends = [att_copy(step) for step in range(1, n_tp)]
    for copy in att_sends:
        copy.start()

    forward(theirs, False)
    loads[4].wait()
    loads[5].wait()
    for step in range(1, n_tp):
        peer = lax.rem(me + step, n_tp)
        pltpu.make_async_remote_copy(
            src_ref=og_hbm,
            dst_ref=og.at[peer],
            send_sem=og_send.at[step],
            recv_sem=og_recv.at[peer],
            device_id={"tp": peer},
            device_id_type=MESH,
        ).wait_recv()
    for piece in range(PIECES):
        wo_arrived(sibling, piece)
        for step in range(1, chips):
            wo_arrived(lax.rem(chip + step, chips) * 2 + 1 - core, piece)

    def norm_and_gate(rows_of, gain_of):
        row_values = rows_of.astype(jnp.float32)
        return (
            jnp.sum(row_values * row_values, axis=-1, keepdims=True),
            (row_values * gain_of).astype(jnp.bfloat16),
        )

    squares, gated = norm_and_gate(att[me], og[me])
    summed = jnp.dot(gated, wo[me], preferred_element_type=jnp.float32)
    for step in range(1, n_tp):
        peer = lax.rem(me + step, n_tp)
        pltpu.make_async_remote_copy(
            src_ref=att.at[peer],
            dst_ref=got.at[peer],
            send_sem=att_send.at[step],
            recv_sem=att_recv.at[peer],
            device_id={"tp": peer},
            device_id_type=MESH,
        ).wait_recv()
        more, gated = norm_and_gate(got[peer], og[peer])
        squares = squares + more
        summed = summed + jnp.dot(gated, wo[peer], preferred_element_type=jnp.float32)
    norm = lax.rsqrt(squares / (channels * n_tp) + EPS)
    out_ref[...] = (summed * norm).astype(jnp.bfloat16)

    for copy in wo_sends + og_sends + att_sends + forwards:
        copy.wait_send()
    if helped:

        @pl.when(z == 1)
        def _():
            relay(0, 0).wait_send()
            relay(0, 1).wait_send()
            for copy in send_back(1, 1, 3) + send_back(0, 1, 2):
                copy.wait_send()

        @pl.when((z == 0) | (z == 2))
        def _():
            relay(0, 0).wait_send()
            relay(1, 0).wait_send()

        @pl.when(z == 2)
        def _():
            ship(1, 0, 1).wait_send()
            for copy in send_back(1, 0, 3):
                copy.wait_send()

        @pl.when(z == 3)
        def _():
            ship(1, 1, 1).wait_send()
            ship(0, 1, 2).wait_send()

    else:
        for distance in range(reach):

            @pl.when(has_next & (z >= distance))
            def _():
                for part in both:
                    relay(part, distance).wait_send()


def on_device(n_grp, n_sp, n_tp, tokens, norm_gain, w_query, w_key, w_value, out_gain, w_out):
    rows, width = tokens.shape
    channels = w_query.shape[1]
    lanes = channels // 2
    heads = lanes // HEAD_DIM
    share = rows // n_tp
    reach = min(-(-REACH // rows), n_sp - 1)
    hbm = pl.BlockSpec(memory_space=pl.ANY)
    vmem = pl.BlockSpec(memory_space=pltpu.VMEM)
    dma = pltpu.SemaphoreType.DMA
    bf16, f32 = jnp.bfloat16, jnp.float32
    return pl.pallas_call(
        functools.partial(kernel, n_grp, n_sp, n_tp, reach),
        out_shape=jax.ShapeDtypeStruct((share, w_out.shape[1]), bf16),
        in_specs=[hbm, vmem, hbm, hbm, hbm, hbm, hbm],
        out_specs=vmem,
        scratch_shapes=[
            pltpu.VMEM((rows, width), bf16),
            pltpu.VMEM((rows, width), bf16),
            pltpu.VMEM((width, channels), bf16),
            pltpu.VMEM((width, channels), bf16),
            pltpu.VMEM((width, channels), bf16),
            pltpu.VMEM((n_tp, 1, channels), f32),
            pltpu.VMEM((n_tp,) + w_out.shape, bf16),
            pltpu.VMEM((2, rows, lanes), bf16),
            pltpu.VMEM((2, reach + 1, 2, rows, lanes), bf16),
            pltpu.VMEM((2, rows, lanes), bf16),
            pltpu.VMEM((4, heads, rows, 1), f32),
            pltpu.VMEM((4, heads, rows, 1), f32),
            pltpu.VMEM((4, rows, lanes), f32),
            pltpu.VMEM((2, rows, lanes), bf16),
            pltpu.VMEM((2, 8, rows), f32),
            pltpu.VMEM((2, rows, lanes), bf16),
            pltpu.VMEM((2, 8, rows), f32),
            pltpu.VMEM((n_tp, share, channels), bf16),
            pltpu.VMEM((n_tp, share, channels), bf16),
            dma((6,)),
            dma((2, reach + 1)),
            dma((2, reach + 1)),
            dma((2,)),
            dma((2,)),
            dma((2, 2)),
            dma((2, 2)),
            dma((n_tp // 2, PIECES)),
            dma((n_tp, PIECES)),
            dma((n_tp // 2, PIECES)),
            dma((n_tp // 2, PIECES)),
            dma((n_tp,)),
            dma((n_tp,)),
            dma((n_tp,)),
            dma((n_tp,)),
        ],
        compiler_params=pltpu.CompilerParams(
            collective_id=0, has_side_effects=True, vmem_limit_bytes=60 * 1024 * 1024
        ),
    )(tokens, norm_gain[None, :], w_query, w_key, w_value, out_gain[None, :], w_out)


def solution(mesh):
    in_specs = (
        P(("grp", "sp"), None),
        P(),
        P(None, "tp"),
        P(None, "tp"),
        P(None, "tp"),
        P("tp"),
        P("tp", None),
    )
    out_specs = P(("grp", "sp", "tp"), None)
    return jax.shard_map(
        functools.partial(on_device, mesh.shape["grp"], mesh.shape["sp"], mesh.shape["tp"]),
        mesh=mesh,
        in_specs=in_specs,
        out_specs=out_specs,
        check_vma=False,
    )
```

time: 43 us -> 37.8 us (0.88)
  the two profiles are of different devices: /device:TPU:29 before, /device:TPU:9 now
where the time goes in v2:
time: 37.8 us; the launch traced here: 37.6 us
  Pallas kernels  35.9 us (95%)
  local copies, waits for them, and re-layouts  1.77 us (5%)
    pallas_call x1, Pallas kernels, on_device(): pl.pallas_call(functools.partial(kernel, n_grp, n_sp, n_tp, reach), out_s...  35.9 us
    unnamed x1, local copies, waits for them, and re-layouts  1.77 us

profile of v2, /device:TPU:9, one launch (start us, length us, event | category | flops | bytes accessed | tf_op | source)
XLA Modules:
  0.0 37.6 jit_solution(2832395385410828611)
XLA Ops:
  0.0 35.9 %shard_map.73 = bf16[96,2048]{1,0:T(8,128)(2,1)} custom-call(bf16[384,2048]{1,0:T(8,128)(2,1)} %tok_hbm.1, f32[1,2048]{1,0:T(1,128)} %bitcast.2, bf16[2048,256]{1,0:T(8,128)(2,1)} %wq_hbm.1, bf16[2048,256]{1,0:T(8,128)(2,1)} %wk_hbm.1, bf16[2048,256]{1,0:T(8,128)(2,1)} %wv_hbm.1, f32[1,256]{1,0:T(1,128)} %bitcast.3, bf16[256,2048]{1,0:T(8,128)(2,1)} %wo_hbm.1), custom_call_target="tpu_custom_call" | custom-call | tf_op jit(solution)/shard_map/pallas_call | solution.py:600
  35.9 1.8 %copy.9 = bf16[96,2048]{1,0:T(8,128)(2,1)} copy(bf16[96,2048]{1,0:T(8,128)(2,1)} %shard_map.73) | data formatting | bytes 786432

commit v3 on v2

--- a/solution.py
+++ b/solution.py
@@ -65,6 +65,7 @@
     query,
     kv,
     guest,
+    allowed,
     top,
     total,
     partial,
@@ -138,6 +139,14 @@
         def _():
             pl.semaphore_signal(barrier, inc=1, device_id={"sp": z + hop}, device_id_type=MESH)
 
+    def mark(distances):
+        for distance in distances:
+            for first in range(0, rows, ROW_BLOCK):
+                allowed[distance, pl.ds(first, ROW_BLOCK), :] = log_multiplicity(
+                    ROW_BLOCK, rows, first + distance * rows
+                )
+
+    mark(range(1))
     neighbours = (z > 0).astype(jnp.int32) + has_next.astype(jnp.int32)
     if helped:
         neighbours = neighbours + (z == 3).astype(jnp.int32) + (z == 1).astype(jnp.int32)
@@ -293,6 +302,7 @@
             ship(1, 1, 1).start()
             ship(0, 1, 2).start()
 
+    mark(range(1, reach + 1))
     lane_head = lax.broadcasted_iota(jnp.int32, (ROW_BLOCK, lanes), 1) // HEAD_DIM
     factor = HEAD_DIM ** (-0.5) * math.log2(math.e)
 
@@ -304,47 +314,54 @@
             )
         return result
 
+    def stacked(rows_of):
+        return jnp.concatenate(
+            [jnp.where(lane_head == head, rows_of, jnp.zeros_like(rows_of)) for head in range(heads)],
+            axis=0,
+        )
+
+    ones = jnp.ones((rows, lanes), jnp.bfloat16)
+
+    def by_head(tall):
+        result = tall[:ROW_BLOCK]
+        for head in range(1, heads):
+            result = jnp.where(
+                lane_head == head, tall[head * ROW_BLOCK : (head + 1) * ROW_BLOCK], result
+            )
+        return result
+
     def attend(parts, state_of, queries_of, slot, distance, fresh):
-        for first in range(0, rows, ROW_BLOCK):
-            cols = min(rows, first + ROW_BLOCK) if distance == 0 else rows
-            first_lag = first + distance * rows
-            if first_lag - (cols - 1) > REACH:
-                continue
-            block = pl.ds(first, ROW_BLOCK)
-            bias = log_multiplicity(ROW_BLOCK, cols, first_lag)
-            for part in parts:
-                state = state_of(part)
-                q_rows = queries_of(part)[block, :]
-                key_rows = kv[part, slot, 0, :cols, :]
-                value_rows = kv[part, slot, 1, :cols, :]
-                mixed, shrinks = None, []
+        for part in parts:
+            state = state_of(part)
+            for first in range(0, rows, ROW_BLOCK):
+                cols = min(rows, first + ROW_BLOCK) if distance == 0 else rows
+                if first + distance * rows - (cols - 1) > REACH:
+                    continue
+                block = pl.ds(first, ROW_BLOCK)
+                scores = lax.dot_general(
+                    stacked(queries_of(part)[block, :]),
+                    kv[part, slot, 0, :cols, :],
+                    (((1,), (1,)), ((), ())),
+                    preferred_element_type=jnp.float32,
+                )
+                bias = allowed[distance, block, :cols]
+                scores = scores * factor + jnp.concatenate([bias] * heads, axis=0)
+                peak = jnp.max(scores, axis=-1, keepdims=True)
+                if not fresh:
+                    old = jnp.concatenate([top[state, head, block, :] for head in range(heads)], axis=0)
+                    peak = jnp.maximum(peak, old)
+                    shrink = by_head(jnp.broadcast_to(jnp.exp2(old - peak), (heads * ROW_BLOCK, lanes)))
                 for head in range(heads):
-                    q_head = jnp.where(lane_head == head, q_rows, jnp.zeros_like(q_rows))
-                    scores = lax.dot_general(
-                        q_head,
-                        key_rows,
-                        (((1,), (1,)), ((), ())),
-                        preferred_element_type=jnp.float32,
-                    )
-                    scores = scores * factor + bias
-                    peak = jnp.max(scores, axis=-1, keepdims=True)
-                    if not fresh:
-                        old = top[state, head, block, :]
-                        peak = jnp.maximum(peak, old)
-                        shrinks.append(jnp.exp2(old - peak))
-                    weights = jnp.exp2(scores - peak)
-                    sums = jnp.sum(weights, axis=-1, keepdims=True)
-                    if not fresh:
-                        sums = sums + shrinks[head] * total[state, head, block, :]
-                    top[state, head, block, :] = peak
-                    total[state, head, block, :] = sums
-                    product = jnp.dot(
-                        weights.astype(jnp.bfloat16), value_rows, preferred_element_type=jnp.float32
-                    )
-                    mixed = product if mixed is None else jnp.where(lane_head == head, product, mixed)
+                    top[state, head, block, :] = peak[head * ROW_BLOCK : (head + 1) * ROW_BLOCK]
+                weights = jnp.exp2(scores - peak).astype(jnp.bfloat16)
+                extended = jnp.concatenate([kv[part, slot, 1, :cols, :], ones[:cols]], axis=1)
+                product = jnp.dot(weights, extended, preferred_element_type=jnp.float32)
+                mixed, sums = by_head(product[:, :lanes]), by_head(product[:, lanes:])
                 if not fresh:
-                    mixed = mixed + spread(shrinks) * partial[state, block, :]
+                    mixed = mixed + shrink * partial[state, block, :]
+                    sums = sums + shrink * total[state, block, :]
                 partial[state, block, :] = mixed
+                total[state, block, :] = sums
 
     def own(parts, distance):
         attend(parts, lambda part: part, lambda part: query.at[part], distance, distance, distance == 0)
@@ -362,11 +379,11 @@
         ).astype(jnp.float32)
         for first in range(0, rows, ROW_BLOCK):
             block = pl.ds(first, ROW_BLOCK)
-            sums = [total[state, head, block, :] for head in range(heads)]
-            help_att[guest_slot, block, :] = (partial[state, block, :] / spread(sums)).astype(jnp.bfloat16)
+            sums = total[state, block, :]
+            help_att[guest_slot, block, :] = (partial[state, block, :] / sums).astype(jnp.bfloat16)
             logs = jnp.zeros((ROW_BLOCK, 128), jnp.float32)
             for head in range(heads):
-                column = top[state, head, block, :] + jnp.log2(sums[head])
+                column = top[state, head, block, :] + jnp.log2(sums[:, head * HEAD_DIM : head * HEAD_DIM + 1])
                 logs = jnp.where(lane == head, jnp.broadcast_to(column, (ROW_BLOCK, 128)), logs)
             help_lse[guest_slot, :, block] = lax.dot_general(
                 pick,
@@ -400,10 +417,12 @@
                 peak = jnp.maximum(column, old)
                 before.append(jnp.exp2(old - peak))
                 after.append(jnp.exp2(column - peak))
-                total[part, head, block, :] = total[part, head, block, :] * before[head] + after[head]
-            partial[part, block, :] = partial[part, block, :] * spread(before) + back_att[
-                part, block, :
-            ].astype(jnp.float32) * spread(after)
+            wide_before, wide_after = spread(before), spread(after)
+            total[part, block, :] = total[part, block, :] * wide_before + wide_after
+            partial[part, block, :] = (
+                partial[part, block, :] * wide_before
+                + back_att[part, block, :].astype(jnp.float32) * wide_after
+            )
 
     both = (0, 1)
     if helped:
@@ -489,19 +508,11 @@
             device_id_type=MESH,
         )
 
-    spread_head = lax.broadcasted_iota(jnp.int32, (share, lanes), 1) // HEAD_DIM
     for target in range(n_tp):
         piece = pl.ds(target * share, share)
         for part in both:
-            denominator = jnp.broadcast_to(total[part, 0, piece, :], (share, lanes))
-            for head in range(1, heads):
-                denominator = jnp.where(
-                    spread_head == head,
-                    jnp.broadcast_to(total[part, head, piece, :], (share, lanes)),
-                    denominator,
-                )
             att[target, :, part * lanes : (part + 1) * lanes] = (
-                partial[part, piece, :] / denominator
+                partial[part, piece, :] / total[part, piece, :]
             ).astype(jnp.bfloat16)
     att_sends = [att_copy(step) for step in range(1, n_tp)]
     for copy in att_sends:
@@ -613,8 +624,9 @@
             pltpu.VMEM((2, rows, lanes), bf16),
             pltpu.VMEM((2, reach + 1, 2, rows, lanes), bf16),
             pltpu.VMEM((2, rows, lanes), bf16),
+            pltpu.VMEM((reach + 1, rows, rows), f32),
             pltpu.VMEM((4, heads, rows, 1), f32),
-            pltpu.VMEM((4, heads, rows, 1), f32),
+            pltpu.VMEM((4, rows, lanes), f32),
             pltpu.VMEM((4, rows, lanes), f32),
             pltpu.VMEM((2, rows, lanes), bf16),
             pltpu.VMEM((2, 8, rows), f32),

time: 37.8 us -> 33.2 us (0.88)
  Pallas kernels: 35.9 us -> 31.2 us
    pallas_call x1, Pallas kernels: 35.9 us -> 31.2 us  [on_device(): pl.pallas_call(functools.partial(kernel, n_grp, n_sp, n_tp, reach), out_s...]
where the time goes in v3:
time: 33.2 us; the launch traced here: 33 us
  Pallas kernels  31.2 us (94%)
  local copies, waits for them, and re-layouts  1.77 us (5%)
    pallas_call x1, Pallas kernels, on_device(): pl.pallas_call(functools.partial(kernel, n_grp, n_sp, n_tp, reach), out_s...  31.2 us
    unnamed x1, local copies, waits for them, and re-layouts  1.77 us

profile of v3, /device:TPU:9, one launch (start us, length us, event | category | flops | bytes accessed | tf_op | source)
XLA Modules:
  0.0 33.0 jit_solution(10806772076785700102)
XLA Ops:
  0.0 31.2 %shard_map.73 = bf16[96,2048]{1,0:T(8,128)(2,1)} custom-call(bf16[384,2048]{1,0:T(8,128)(2,1)} %tok_hbm.1, f32[1,2048]{1,0:T(1,128)} %bitcast.2, bf16[2048,256]{1,0:T(8,128)(2,1)} %wq_hbm.1, bf16[2048,256]{1,0:T(8,128)(2,1)} %wk_hbm.1, bf16[2048,256]{1,0:T(8,128)(2,1)} %wv_hbm.1, f32[1,256]{1,0:T(1,128)} %bitcast.3, bf16[256,2048]{1,0:T(8,128)(2,1)} %wo_hbm.1), custom_call_target="tpu_custom_call" | custom-call | tf_op jit(solution)/shard_map/pallas_call | solution.py:611
  31.2 1.8 %copy.9 = bf16[96,2048]{1,0:T(8,128)(2,1)} copy(bf16[96,2048]{1,0:T(8,128)(2,1)} %shard_map.73) | data formatting | bytes 786432

commit v4 on v3

--- a/solution.py
+++ b/solution.py
@@ -15,7 +15,7 @@
 NEG = -1e30
 MESH = pl.DeviceIdType.MESH
 ROW_BLOCK = 128
-PIECES = 4
+PIECES = 8
 
 
 def log_multiplicity(rows, cols, first_lag):
@@ -427,13 +427,12 @@
     both = (0, 1)
     if helped:
 
-        @pl.when(z != 1)
-        def _():
-            own(both, 0)
+        own(both, 0)
+        early = own_pieces // 2
+        forward(mine[:early], paired)
 
         @pl.when(z == 1)
         def _():
-            own(both, 0)
             arrived(0, 1)
             relay(0, 1).start()
             guest_arrived(1)
@@ -442,7 +441,19 @@
             help_out(1, 0, 0, 1, True)
             own([0], 1)
 
-        forward(mine[:1], paired)
+        @pl.when(z == 2)
+        def _():
+            arrived(0, 1)
+            guest_arrived(1)
+            help_out(0, 1, 1, 2, True)
+            own([0], 1)
+
+        @pl.when(z == 3)
+        def _():
+            arrived(0, 1)
+            own([0], 1)
+
+        forward(mine[early:], paired)
 
         @pl.when(z == 1)
         def _():
@@ -455,15 +466,6 @@
 
         @pl.when(z == 2)
         def _():
-            arrived(0, 1)
-            guest_arrived(1)
-            help_out(0, 1, 1, 2, True)
-            own([0], 1)
-
-        forward(mine[1:], paired)
-
-        @pl.when(z == 2)
-        def _():
             arrived(0, 2)
             help_out(0, 1, 2, 3, False)
             give_back(1, 0, 3)
@@ -472,8 +474,6 @@
 
         @pl.when(z == 3)
         def _():
-            arrived(0, 1)
-            own([0], 1)
             arrived(1, 1)
             own([1], 1)
             take_back(1)

time: 33.2 us -> 32.6 us (0.982)
  the two profiles are of different devices: /device:TPU:9 before, /device:TPU:19 now
where the time goes in v4:
time: 32.6 us; the launch traced here: 32.4 us
  Pallas kernels  30.6 us (94%)
  local copies, waits for them, and re-layouts  1.77 us (5%)
    pallas_call x1, Pallas kernels, on_device(): pl.pallas_call(functools.partial(kernel, n_grp, n_sp, n_tp, reach), out_s...  30.6 us
    unnamed x1, local copies, waits for them, and re-layouts  1.77 us

profile of v4, /device:TPU:19, one launch (start us, length us, event | category | flops | bytes accessed | tf_op | source)
XLA Modules:
  0.0 32.4 jit_solution(14234819408371624823)
XLA Ops:
  0.0 30.6 %shard_map.73 = bf16[96,2048]{1,0:T(8,128)(2,1)} custom-call(bf16[384,2048]{1,0:T(8,128)(2,1)} %tok_hbm.1, f32[1,2048]{1,0:T(1,128)} %bitcast.2, bf16[2048,256]{1,0:T(8,128)(2,1)} %wq_hbm.1, bf16[2048,256]{1,0:T(8,128)(2,1)} %wk_hbm.1, bf16[2048,256]{1,0:T(8,128)(2,1)} %wv_hbm.1, f32[1,256]{1,0:T(1,128)} %bitcast.3, bf16[256,2048]{1,0:T(8,128)(2,1)} %wo_hbm.1), custom_call_target="tpu_custom_call" | custom-call | tf_op jit(solution)/shard_map/pallas_call | solution.py:611
  30.6 1.8 %copy.9 = bf16[96,2048]{1,0:T(8,128)(2,1)} copy(bf16[96,2048]{1,0:T(8,128)(2,1)} %shard_map.73) | data formatting | bytes 786432
